TPU v7x, 32 devices: a whole 2x2x4 slice. The times are simulated.
32 devices in a mesh: sp: 8 (over z, y), dp: 4 (over x, core).
Axes of the slice: x: 2, y: 2, z: 4, core: 2. Of those that a mesh axis runs over, the one named last changes fastest.
Arguments:
- residual: bfloat16 [4, 1024, 2048], P('dp', 'sp'), may hold values from -6 to 6
- query_maps: bfloat16 [4, 1024, 2048], P('dp', 'sp'), may hold values from -200 to 200
- key_maps: bfloat16 [4, 1024, 2048], P('dp', 'sp'), may hold values from -200 to 200
- value_rows: bfloat16 [4, 1024, 2048], P('dp', 'sp'), may hold values from -6 to 6
- lambdas: float32 [16], replicated, may hold values from 0.3 to 0.8
- head_gain: float32 [2048], replicated, may hold values from 0.1 to 1.9
- out_weight: bfloat16 [2048, 2048], replicated, may hold values from -0.125 to 0.125
- ffn_gain: float32 [2048], replicated, may hold values from 0.1 to 1.9
- routes: int32 [4, 1024, 2], P('dp', 'sp'), may hold values from 0 to 31, all different within a row; in each aligned block of 128 rows (0 to 127, 128 to 255, ..., all dimensions but the last counted through in order) at most 16 rows name the same one
- route_weights: float32 [4, 1024, 2], P('dp', 'sp'), may hold values from 0.2 to 1
- expert_gate: bfloat16 [32, 2048, 1024], P(('sp', 'dp')), may hold values from -0.125 to 0.125
- expert_up: bfloat16 [32, 2048, 1024], P(('sp', 'dp')), may hold values from -0.125 to 0.125
- expert_down: bfloat16 [32, 1024, 2048], P(('sp', 'dp')), may hold values from -0.1875 to 0.1875
Outputs:
- layer_out: bfloat16 [4, 1024, 2048], P('dp', 'sp')
Inputs may be any that keep to these rules, and one draw needn't show every extreme that they name: `routes`: A token's 2 experts differ; among the 128 rows of one device no expert is named more than 16 times, and in every draw some expert is named exactly 16 times by one device's rows.
All inputs are finite; a program needn't handle non-finite values.
Results may differ from a plain program's by a relative error of at most 0.012.
Values may be sent and summed in bfloat16 or wider, within the bound.
A program may use at most 128 MiB of HBM per device.

v0:
```python
import functools
import math

import jax
import jax.numpy as jnp
from jax import lax
from jax.experimental import pallas as pl
from jax.experimental.pallas import tpu as pltpu
from jax.sharding import PartitionSpec as P

D = 2048
HEADS = 16
HD = 64
VD = 128


eps = 1e-06


def attend_head(query_head, key_head, value_head, lam_head, gain_head):
    length = query_head.shape[0]
    block_rows = min(512, length)
    count_blocks = length // block_rows
    scaling = query_head.shape[-1] ** (-0.5)
    query_blocks = query_head.reshape(count_blocks, block_rows, 2, query_head.shape[-1])

    def one_block(query_block):
        scores = (
            jnp.einsum("qmd,kmd->mqk", query_block, key_head, preferred_element_type=jnp.float32)
            * scaling
        )
        probabilities = jax.nn.softmax(scores, axis=-1)
        mixed_map = (probabilities[0] - lam_head * probabilities[1]).astype(jnp.bfloat16)
        head_out = jnp.dot(mixed_map, value_head, preferred_element_type=jnp.float32)
        normed = head_out * lax.rsqrt(jnp.mean(head_out * head_out, axis=-1, keepdims=True) + eps)
        return (normed * gain_head * 0.8).astype(jnp.bfloat16)

    return lax.map(one_block, query_blocks).reshape(length, value_head.shape[-1])


def on_device(
    residual,
    query_maps,
    key_maps,
    value_rows,
    lambdas,
    head_gain,
    out_weight,
    ffn_gain,
    routes,
    route_weights,
    expert_gate,
    expert_up,
    expert_down,
):
    count_sp = lax.axis_size("sp")
    count_dp = lax.axis_size("dp")
    heads_here = HEADS // count_sp
    queries, keys_all, values_all = (
        lax.all_to_all(query_maps, "sp", split_axis=2, concat_axis=1, tiled=True),
        lax.all_to_all(key_maps, "sp", split_axis=2, concat_axis=1, tiled=True),
        lax.all_to_all(value_rows, "sp", split_axis=2, concat_axis=1, tiled=True),
    )
    first_head = lax.axis_index("sp") * heads_here
    lam_here = lax.dynamic_slice_in_dim(lambdas, first_head, heads_here)
    gain_here = lax.dynamic_slice_in_dim(head_gain, first_head * VD, heads_here * VD)
    outputs = []
    for head_index in range(heads_here):
        query_head = queries[0, :, head_index * 2 * HD : (head_index + 1) * 2 * HD].reshape(
            -1, 2, HD
        )
        key_head = keys_all[0, :, head_index * 2 * HD : (head_index + 1) * 2 * HD].reshape(
            -1, 2, HD
        )
        value_head = values_all[0, :, head_index * VD : (head_index + 1) * VD]
        gain_head = gain_here[head_index * VD : (head_index + 1) * VD]
        outputs.append(
            attend_head(query_head, key_head, value_head, lam_here[head_index], gain_head)
        )
    attended = jnp.concatenate(outputs, axis=1)[None]
    returned_heads = lax.all_to_all(attended, "sp", split_axis=1, concat_axis=2, tiled=True)
    projected = jnp.dot(returned_heads[0], out_weight, preferred_element_type=jnp.float32)
    residual_mid = (residual[0].astype(jnp.float32) + projected).astype(jnp.bfloat16)
    middle = residual_mid.astype(jnp.float32)
    expert_input = (
        middle * lax.rsqrt(jnp.mean(middle * middle, axis=-1, keepdims=True) + eps) * ffn_gain
    ).astype(jnp.bfloat16)
    tok_rows = residual.shape[1]
    experts_all = count_sp * count_dp
    capacity = max(2, 4 * tok_rows // experts_all)
    flat_routes = routes[0].reshape(-1)
    flat_weights = route_weights[0].reshape(-1)
    onehot = (flat_routes[:, None] == jnp.arange(experts_all, dtype=jnp.int32)[None, :]).astype(
        jnp.int32
    )
    before = jnp.cumsum(onehot, axis=0) - onehot
    rank_of = jnp.sum(before * onehot, axis=1)
    slot = flat_routes * capacity + rank_of
    token_of = jnp.arange(flat_routes.shape[0], dtype=jnp.int32) // routes.shape[2]
    slot_token = jnp.full((experts_all * capacity,), tok_rows, jnp.int32).at[slot].set(token_of)
    padded_input = jnp.concatenate([expert_input, jnp.zeros((1, D), jnp.bfloat16)], axis=0)
    buffer = padded_input[slot_token].reshape(experts_all, capacity, D)
    received = lax.all_to_all(buffer, ("sp", "dp"), split_axis=0, concat_axis=0, tiled=True)
    row_block = received.reshape(-1, D)
    gate_part = jnp.dot(row_block, expert_gate[0], preferred_element_type=jnp.float32)
    up_part = jnp.dot(row_block, expert_up[0], preferred_element_type=jnp.float32)
    hidden = (jax.nn.silu(gate_part) * up_part).astype(jnp.bfloat16)
    expert_out = jnp.dot(hidden, expert_down[0], preferred_element_type=jnp.float32).astype(
        jnp.bfloat16
    )
    returned = lax.all_to_all(
        expert_out.reshape(received.shape), ("sp", "dp"), split_axis=0, concat_axis=0, tiled=True
    )
    picked = returned.reshape(experts_all * capacity, D)[slot]
    weighted = (picked.astype(jnp.float32) * flat_weights[:, None]).reshape(
        tok_rows, routes.shape[2], D
    )
    layer_out = (middle + jnp.sum(weighted, axis=1)).astype(jnp.bfloat16)
    return layer_out[None]


MESH = pl.DeviceIdType.MESH
VMEM_LIMIT = 60 * 1024 * 1024


def slot_masks(routes, first_expert, experts_all, experts_here, capacity):
    rows = routes.shape[1]
    first, second = routes[0:1, :], routes[1:2, :]
    experts = lax.broadcasted_iota(jnp.int32, (experts_all, rows), 0)
    named_first, named_second = experts == first, experts == second
    named = jnp.where(named_first | named_second, 1.0, 0.0).astype(jnp.bfloat16)
    earlier = lax.broadcasted_iota(jnp.int32, (rows, rows), 0) < lax.broadcasted_iota(
        jnp.int32, (rows, rows), 1
    )
    before = jnp.dot(
        named, jnp.where(earlier, 1.0, 0.0).astype(jnp.bfloat16), preferred_element_type=jnp.float32
    )
    slots = lax.broadcasted_iota(jnp.int32, (experts_here * capacity, rows), 0)
    masks = []
    for route, chosen in ((first, named_first), (second, named_second)):
        rank = jnp.sum(jnp.where(chosen, before, 0.0), axis=0, keepdims=True).astype(jnp.int32)
        masks.append(slots == (route - first_expert) * capacity + rank)
    return masks


def mixer_kernel(
    count_sp,
    lam_ref,
    q_ref,
    k_ref,
    v_ref,
    residual_ref,
    gain_ref,
    ow_hbm,
    fgain_ref,
    mid_ref,
    xin_ref,
    qh,
    kh,
    vh,
    outs,
    att,
    ow,
    send_sem,
    recv_sem,
    back_send,
    back_recv,
    local_sem,
    ow_sem,
):
    me = lax.axis_index("sp")
    rows = q_ref.shape[0]
    heads_here = HEADS // count_sp
    length = rows * count_sp
    sources = ((k_ref, kh), (q_ref, qh), (v_ref, vh))

    barrier = pltpu.get_barrier_semaphore()

    def greet(d, carry):
        pl.semaphore_signal(
            barrier, inc=1, device_id={"sp": lax.rem(me + d, count_sp)}, device_id_type=MESH
        )
        return carry

    lax.fori_loop(1, count_sp, greet, 0)
    weight_copy = pltpu.make_async_copy(ow_hbm, ow, ow_sem)
    my_rows = pl.ds(pl.multiple_of(me * rows, rows), rows)

    def local_copy(t, h):
        src, dst = sources[t]
        cols = pl.ds(pl.multiple_of((me * heads_here + h) * VD, VD), VD)
        return pltpu.make_async_copy(src.at[:, cols], dst.at[h, my_rows, :], local_sem.at[t, h])

    def outgoing(t, h, d):
        src, dst = sources[t]
        peer = lax.rem(me + d, count_sp)
        cols = pl.ds(pl.multiple_of((peer * heads_here + h) * VD, VD), VD)
        return pltpu.make_async_remote_copy(
            src_ref=src.at[:, cols],
            dst_ref=dst.at[h, my_rows, :],
            send_sem=send_sem.at[t, h, d],
            recv_sem=recv_sem.at[t, h, d],
            device_id={"sp": peer},
            device_id_type=MESH,
        )

    pl.semaphore_wait(barrier, count_sp - 1)
    for h in range(heads_here):

        for t in (0, 2, 1):

            def start_all(i, carry, t=t, h=h):
                outgoing(t, h, 1 + lax.rem(i + count_sp // 2 - 1, count_sp - 1)).start()
                return carry

            lax.fori_loop(0, count_sp - 1, start_all, 0)
            local_copy(t, h).start()
    weight_copy.start()

    def returning(h, p, d):
        dst_cols = pl.ds(pl.multiple_of((me * heads_here + h) * VD, VD), VD)
        return pltpu.make_async_remote_copy(
            src_ref=outs.at[h, pl.ds(pl.multiple_of(p * rows, rows), rows), :],
            dst_ref=att.at[:, dst_cols],
            send_sem=back_send.at[h, d],
            recv_sem=back_recv.at[h, d],
            device_id={"sp": p},
            device_id_type=MESH,
        )

    factor = HD ** (-0.5) * math.log2(math.e)
    lanes = lax.broadcasted_iota(jnp.int32, (rows, VD), 1)
    for h in range(heads_here):
        for t in range(3):
            local_copy(t, h).wait()
        for t in (0, 2):

            def arrived(d, carry, t=t, h=h):
                outgoing(t, h, d).wait_recv()
                return carry

            lax.fori_loop(1, count_sp, arrived, 0)
        head = me * heads_here + h
        lam = lam_ref[head]
        gain = gain_ref[pl.ds(head, 1), :]

        def attend(p, h=h, lam=lam, gain=gain):
            at = pl.ds(pl.multiple_of(p * rows, rows), rows)
            q = qh[h, at, :]
            zero = jnp.zeros_like(q)
            both = jnp.concatenate(
                [jnp.where(lanes < HD, q, zero), jnp.where(lanes < HD, zero, q)], axis=0
            )
            scores = lax.dot_general(
                both, kh[h], (((1,), (1,)), ((), ())), preferred_element_type=jnp.float32
            )
            top = jnp.max(scores, axis=1, keepdims=True)
            e = jnp.exp2((scores - top) * factor)
            total = jnp.sum(e, axis=1, keepdims=True)
            total_1, total_2 = total[:rows], total[rows:]
            share = lam * total_1 / total_2
            mixed = (e[:rows] - share * e[rows:]).astype(jnp.bfloat16)
            head_out = jnp.dot(mixed, vh[h], preferred_element_type=jnp.float32) / total_1
            normed = head_out * lax.rsqrt(
                jnp.mean(head_out * head_out, axis=-1, keepdims=True) + eps
            )
            return (normed * gain * 0.8).astype(jnp.bfloat16)

        def step(i, carry, h=h, attend=attend):
            d = 1 + lax.rem(i + count_sp // 2 - 1, count_sp - 1)
            p = lax.rem(me + count_sp - d, count_sp)
            outgoing(1, h, d).wait_recv()
            outs[h, pl.ds(pl.multiple_of(p * rows, rows), rows), :] = attend(p)
            returning(h, p, d).start()
            return carry

        lax.fori_loop(0, count_sp - 1, step, 0)
        att[:, pl.ds(pl.multiple_of(head * VD, VD), VD)] = attend(me)

    weight_copy.wait()
    for h in range(heads_here):

        def back(d, carry, h=h):
            returning(h, lax.rem(me + count_sp - d, count_sp), d).wait_recv()
            return carry

        lax.fori_loop(1, count_sp, back, 0)

    tile = 512
    square = jnp.zeros((rows, 1), jnp.float32)
    for j in range(D // tile):
        cols = slice(j * tile, (j + 1) * tile)
        projected = jnp.dot(att[...], ow[:, cols], preferred_element_type=jnp.float32)
        middle = (residual_ref[:, cols].astype(jnp.float32) + projected).astype(jnp.bfloat16)
        mid_ref[:, cols] = middle
        wide = middle.astype(jnp.float32)
        square = square + jnp.sum(wide * wide, axis=1, keepdims=True)
    scale = lax.rsqrt(square / D + eps)
    xin_ref[...] = (mid_ref[...].astype(jnp.float32) * scale * fgain_ref[...]).astype(jnp.bfloat16)

    for h in range(heads_here):

        def drain(d, carry, h=h):
            for t in range(3):
                outgoing(t, h, d).wait_send()
            returning(h, lax.rem(me + count_sp - d, count_sp), d).wait_send()
            return carry

        lax.fori_loop(1, count_sp, drain, 0)


PARTS = 2


def experts_kernel(
    count_sp,
    count_dp,
    capacity,
    xin_ref,
    mid_ref,
    routes_ref,
    weights_ref,
    gate_hbm,
    up_hbm,
    down_hbm,
    out_ref,
    routes_far,
    weights_far,
    xin_far,
    partial,
    far_sum,
    buffer,
    received,
    results,
    returned,
    gate,
    up,
    down,
    hidden,
    far_send,
    far_recv,
    sum_send,
    sum_recv,
    send_sem,
    recv_sem,
    back_send,
    back_recv,
    own_sem,
    weight_sem,
):
    count = count_sp * count_dp
    half = count // 2
    sp = lax.axis_index("sp")
    base = (sp // (count_sp // 2)) * half
    me = sp * count_dp + lax.axis_index("dp") - base
    partner = {"sp": lax.rem(sp + count_sp // 2, count_sp)}
    width = gate.shape[1]
    span = D // PARTS

    def coords(p):
        return {"sp": (base + p) // count_dp, "dp": lax.rem(base + p, count_dp)}

    barrier = pltpu.get_barrier_semaphore()

    def greet(d, carry):
        pl.semaphore_signal(
            barrier, inc=1, device_id=coords(lax.rem(me + d, half)), device_id_type=MESH
        )
        return carry

    lax.fori_loop(1, half, greet, 0)
    pl.semaphore_signal(barrier, inc=1, device_id=partner, device_id_type=MESH)

    def rows_of(b, i):
        return pl.ds(pl.multiple_of((b * half + i) * capacity, capacity), capacity)

    def part(c):
        return pl.ds(c * span, span)

    def offset(i):
        return 1 + lax.rem(i + half // 2 - 2, half - 1)

    def to_partner(src, dst, sent, got):
        return pltpu.make_async_remote_copy(
            src_ref=src,
            dst_ref=dst,
            send_sem=sent,
            recv_sem=got,
            device_id=partner,
            device_id_type=MESH,
        )

    far = [
        to_partner(xin_ref.at[:, part(c)], xin_far.at[:, part(c)], far_send.at[c], far_recv.at[c])
        for c in range(PARTS)
    ]
    far.append(to_partner(routes_ref, routes_far, far_send.at[PARTS], far_recv.at[PARTS]))
    far.append(
        to_partner(weights_ref, weights_far, far_send.at[PARTS + 1], far_recv.at[PARTS + 1])
    )
    far_back = [
        to_partner(partial.at[:, part(c)], far_sum.at[:, part(c)], sum_send.at[c], sum_recv.at[c])
        for c in range(PARTS)
    ]

    def outgoing(b, c, i):
        p = lax.rem(me + offset(i), half)
        return pltpu.make_async_remote_copy(
            src_ref=buffer.at[rows_of(b, p), part(c)],
            dst_ref=received.at[rows_of(b, i), part(c)],
            send_sem=send_sem.at[b, c, i],
            recv_sem=recv_sem.at[b, c, i],
            device_id=coords(p),
            device_id_type=MESH,
        )

    def returning(b, c, i):
        p = lax.rem(me + half - offset(i), half)
        return pltpu.make_async_remote_copy(
            src_ref=results.at[rows_of(b, i), part(c)],
            dst_ref=returned.at[rows_of(b, me), part(c)],
            send_sem=back_send.at[b, c, i],
            recv_sem=back_recv.at[b, c, i],
            device_id=coords(p),
            device_id_type=MESH,
        )

    def own_in(b, c):
        return pltpu.make_async_copy(
            buffer.at[rows_of(b, me), part(c)],
            received.at[rows_of(b, 0), part(c)],
            own_sem.at[0, b, c],
        )

    def own_out(b, c):
        return pltpu.make_async_copy(
            results.at[rows_of(b, 0), part(c)],
            returned.at[rows_of(b, me), part(c)],
            own_sem.at[1, b, c],
        )

    loads = [
        pltpu.make_async_copy(src, dst, weight_sem.at[j])
        for j, (src, dst) in enumerate(((gate_hbm, gate), (up_hbm, up), (down_hbm, down)))
    ]

    def each(do):
        def body(i, carry):
            do(i)
            return carry

        lax.fori_loop(1, half, body, 0)

    pl.semaphore_wait(barrier, half)
    far[PARTS].start()
    far[PARTS + 1].start()
    for c in range(PARTS):
        far[c].start()

    def spread(b, c, masks, source):
        picks = jnp.where(masks[0] | masks[1], 1.0, 0.0).astype(jnp.bfloat16)
        block = slice(b * half * capacity, (b + 1) * half * capacity)
        buffer[block, c * span : (c + 1) * span] = jnp.dot(
            picks, source[:, c * span : (c + 1) * span], preferred_element_type=jnp.float32
        ).astype(jnp.bfloat16)
        each(lambda i: outgoing(b, c, i).start())
        own_in(b, c).start()

    def combines(masks, weights):
        combine = (
            jnp.where(masks[0], weights[0:1, :], 0.0) + jnp.where(masks[1], weights[1:2, :], 0.0)
        ).T
        high = combine.astype(jnp.bfloat16)
        return high, (combine - high.astype(jnp.float32)).astype(jnp.bfloat16)

    def combined(pair, b, c):
        block = returned[
            b * half * capacity : (b + 1) * half * capacity, c * span : (c + 1) * span
        ]
        return jnp.dot(pair[0], block, preferred_element_type=jnp.float32) + jnp.dot(
            pair[1], block, preferred_element_type=jnp.float32
        )

    near_masks = slot_masks(routes_ref[...], base, count, half, capacity)
    for c in range(PARTS):
        spread(0, c, near_masks, xin_ref)
    for load in loads:
        load.start()
    near_pair = combines(near_masks, weights_ref[...])

    far[PARTS].wait_recv()
    far[PARTS + 1].wait_recv()
    far_masks = slot_masks(routes_far[...], base, count, half, capacity)
    far_pair = combines(far_masks, weights_far[...])
    for c in range(PARTS):
        far[c].wait_recv()
        spread(1, c, far_masks, xin_far)
    for load in loads:
        load.wait()

    for b in range(2):
        at = slice(b * half * capacity, (b + 1) * half * capacity)
        for c in range(PARTS):
            own_in(b, c).wait()
            each(lambda i, b=b, c=c: outgoing(b, c, i).wait_recv())

        def make_hidden(j, carry, at=at):
            cols = pl.ds(pl.multiple_of(j * 256, 256), 256)
            gate_part = jnp.dot(received[at, :], gate[:, cols], preferred_element_type=jnp.float32)
            up_part = jnp.dot(received[at, :], up[:, cols], preferred_element_type=jnp.float32)
            hidden[:, cols] = (jax.nn.silu(gate_part) * up_part).astype(jnp.bfloat16)
            return carry

        lax.fori_loop(0, width // 256, make_hidden, 0)
        for c in range(PARTS):

            def make_out(j, carry, at=at, c=c):
                cols = pl.ds(pl.multiple_of(c * span + j * 512, 512), 512)
                results[at, cols] = jnp.dot(
                    hidden[...], down[:, cols], preferred_element_type=jnp.float32
                ).astype(jnp.bfloat16)
                return carry

            lax.fori_loop(0, span // 512, make_out, 0)
            if b == 1:
                each(lambda i, c=c: returning(1, c, i).start())
    for b in (1, 0):
        for c in range(PARTS):
            own_out(b, c).start()
    for c in range(PARTS):
        each(lambda i, c=c: returning(0, c, i).start())

    for c in range(PARTS):
        own_out(1, c).wait()
        each(lambda i, c=c: returning(1, c, i).wait_recv())
        partial[:, c * span : (c + 1) * span] = combined(far_pair, 1, c).astype(jnp.bfloat16)
        far_back[c].start()
    for c in range(PARTS):
        own_out(0, c).wait()
        each(lambda i, c=c: returning(0, c, i).wait_recv())
        near = combined(near_pair, 0, c)
        far_back[c].wait_recv()
        cols = slice(c * span, (c + 1) * span)
        out_ref[:, cols] = (
            mid_ref[:, cols].astype(jnp.float32) + near + far_sum[:, cols].astype(jnp.float32)
        ).astype(jnp.bfloat16)

    for copy in far + far_back:
        copy.wait_send()

    def drain(i):
        for b in range(2):
            for c in range(PARTS):
                outgoing(b, c, i).wait_send()
                returning(b, c, i).wait_send()

    each(drain)


def kernels_on_device(
    residual,
    query_maps,
    key_maps,
    value_rows,
    lambdas,
    head_gain,
    out_weight,
    ffn_gain,
    routes,
    route_weights,
    expert_gate,
    expert_up,
    expert_down,
):
    count_sp = lax.axis_size("sp")
    count_dp = lax.axis_size("dp")
    experts_all = count_sp * count_dp
    rows = residual.shape[1]
    capacity = max(2, 4 * rows // experts_all)
    if capacity % 16 or count_sp % 2:
        return on_device(
            residual,
            query_maps,
            key_maps,
            value_rows,
            lambdas,
            head_gain,
            out_weight,
            ffn_gain,
            routes,
            route_weights,
            expert_gate,
            expert_up,
            expert_down,
        )
    heads_here = HEADS // count_sp
    slots = experts_all * capacity
    vmem = pl.BlockSpec(memory_space=pltpu.VMEM)
    hbm = pl.BlockSpec(memory_space=pl.ANY)
    dma = pltpu.SemaphoreType.DMA
    bf16 = jnp.bfloat16
    length = rows * count_sp
    middle, expert_input = pl.pallas_call(
        functools.partial(mixer_kernel, count_sp),
        out_shape=(
            jax.ShapeDtypeStruct((rows, D), bf16),
            jax.ShapeDtypeStruct((rows, D), bf16),
        ),
        in_specs=[pl.BlockSpec(memory_space=pltpu.SMEM), hbm, hbm, hbm, vmem, vmem, hbm, vmem],
        out_specs=(vmem, vmem),
        scratch_shapes=[
            pltpu.VMEM((heads_here, length, VD), bf16),
            pltpu.VMEM((heads_here, length, VD), bf16),
            pltpu.VMEM((heads_here, length, VD), bf16),
            pltpu.VMEM((heads_here, length, VD), bf16),
            pltpu.VMEM((rows, HEADS * VD), bf16),
            pltpu.VMEM(out_weight.shape, bf16),
            dma((3, heads_here, count_sp)),
            dma((3, heads_here, count_sp)),
            dma((heads_here, count_sp)),
            dma((heads_here, count_sp)),
            dma((3, heads_here)),
            dma,
        ],
        compiler_params=pltpu.CompilerParams(
            collective_id=0, has_side_effects=True, vmem_limit_bytes=VMEM_LIMIT
        ),
    )(
        lambdas,
        query_maps[0],
        key_maps[0],
        value_rows[0],
        residual[0],
        head_gain.reshape(HEADS, VD),
        out_weight,
        ffn_gain.reshape(1, D),
    )
    width = expert_gate.shape[2]
    out = pl.pallas_call(
        functools.partial(experts_kernel, count_sp, count_dp, capacity),
        out_shape=jax.ShapeDtypeStruct((rows, D), bf16),
        in_specs=[vmem, vmem, vmem, vmem, hbm, hbm, hbm],
        out_specs=vmem,
        scratch_shapes=[
            pltpu.VMEM((routes.shape[2], rows), jnp.int32),
            pltpu.VMEM((routes.shape[2], rows), jnp.float32),
            pltpu.VMEM((rows, D), bf16),
            pltpu.VMEM((rows, D), bf16),
            pltpu.VMEM((rows, D), bf16),
            pltpu.VMEM((slots, D), bf16),
            pltpu.VMEM((slots, D), bf16),
            pltpu.VMEM((slots, D), bf16),
            pltpu.VMEM((slots, D), bf16),
            pltpu.VMEM((D, width), bf16),
            pltpu.VMEM((D, width), bf16),
            pltpu.VMEM((width, D), bf16),
            pltpu.VMEM((slots // 2, width), bf16),
            dma((PARTS + 2,)),
            dma((PARTS + 2,)),
            dma((PARTS,)),
            dma((PARTS,)),
            dma((2, PARTS, experts_all // 2)),
            dma((2, PARTS, experts_all // 2)),
            dma((2, PARTS, experts_all // 2)),
            dma((2, PARTS, experts_all // 2)),
            dma((2, 2, PARTS)),
            dma((3,)),
        ],
        compiler_params=pltpu.CompilerParams(
            collective_id=1, has_side_effects=True, vmem_limit_bytes=VMEM_LIMIT
        ),
    )(
        expert_input,
        middle,
        routes[0].T,
        route_weights[0].T,
        expert_gate[0],
        expert_up[0],
        expert_down[0],
    )
    return out[None]


def solution(mesh):
    return jax.shard_map(
        kernels_on_device,
        mesh=mesh,
        in_specs=(
            P("dp", "sp", None),
            P("dp", "sp", None),
            P("dp", "sp", None),
            P("dp", "sp", None),
            P(),
            P(),
            P(),
            P(),
            P("dp", "sp", None),
            P("dp", "sp", None),
            P(("sp", "dp"), None, None),
            P(("sp", "dp"), None, None),
            P(("sp", "dp"), None, None),
        ),
        out_specs=P("dp", "sp", None),
        check_vma=False,
    )
```

profile of v0, /device:TPU:0, one launch (start us, length us, event | category | flops | bytes accessed | tf_op | source)
XLA Modules:
  0.0 143.8 jit_solution(3414158005332134828)
XLA Ops:
  0.0 56.5 %shard_map.127 = (bf16[128,2048]{1,0:T(8,128)(2,1)}, bf16[128,2048]{1,0:T(8,128)(2,1)}) custom-call(f32[16]{0:T(128)} %lam_ref.1, bf16[128,2048]{1,0:T(8,128)(2,1)} %bitcast.20, bf16[128,2048]{1,0:T(8,128)(2,1)} %bitcast.21, bf16[128,2048]{1,0:T(8,128)(2,1)} %bitcast.22, bf16[128,2048]{1,0:T(8,128)(2,1)} %bitcast.23, f32[16,128]{1,0:T(8,128)} %bitcast.24, ...), custom_call_target="tpu_custom_call" | custom-call | tf_op jit(solution)/shard_map/pallas_call | solution.py:603
  56.5 85.4 %shard_map.128 = bf16[128,2048]{1,0:T(8,128)(2,1)} custom-call(bf16[128,2048]{1,0:T(8,128)(2,1)} %get-tuple-element.7.xin_ref, bf16[128,2048]{1,0:T(8,128)(2,1)} %get-tuple-element.8.mid_ref, s32[2,128]{1,0:T(2,128)} %bitcast.26, f32[2,128]{1,0:T(2,128)} %bitcast.27, bf16[2048,1024]{1,0:T(8,128)(2,1)} %bitcast.16, bf16[2048,1024]{1,0:T(8,128)(2,1)} %bitcast.17, ...), custom_call_target="tpu_custom_call" | custom-call | tf_op jit(solution)/shard_map/pallas_call | solution.py:639
  142.0 1.9 %copy.15 = bf16[1,128,2048]{2,1,0:T(8,128)(2,1)} copy(bf16[1,128,2048]{2,1,0:T(8,128)(2,1)} %bitcast.19) | data formatting | bytes 1048576
where the time goes:
time: 144 us
  Pallas kernels  142 us (99%)
  local copies, waits for them, and re-layouts  1.88 us (1%)
    pallas_call x1, Pallas kernels, kernels_on_device(): pl.pallas_call(functools.partial(experts_kernel, count_sp, count_dp, capa...  85.4 us
    pallas_call x1, Pallas kernels, kernels_on_device(): pl.pallas_call(functools.partial(mixer_kernel, count_sp), out_shape=(jax....  56.5 us

commit v1 on v0

--- a/solution.py
+++ b/solution.py
@@ -309,7 +309,8 @@
         lax.fori_loop(1, count_sp, drain, 0)
 
 
-PARTS = 2
+PARTS = 4
+LINE = 4
 
 
 def experts_kernel(
@@ -328,7 +329,8 @@
     weights_far,
     xin_far,
     partial,
-    far_sum,
+    inbox,
+    near_sum,
     buffer,
     received,
     results,
@@ -337,8 +339,10 @@
     up,
     down,
     hidden,
-    far_send,
-    far_recv,
+    table_send,
+    table_recv,
+    line_send,
+    line_recv,
     sum_send,
     sum_recv,
     send_sem,
@@ -349,210 +353,331 @@
     weight_sem,
 ):
     count = count_sp * count_dp
-    half = count // 2
+    inner = count_sp // LINE
+    peers = inner * count_dp
     sp = lax.axis_index("sp")
-    base = (sp // (count_sp // 2)) * half
-    me = sp * count_dp + lax.axis_index("dp") - base
-    partner = {"sp": lax.rem(sp + count_sp // 2, count_sp)}
+    z, y = sp // inner, lax.rem(sp, inner)
+    me = y * count_dp + lax.axis_index("dp")
     width = gate.shape[1]
     span = D // PARTS
-
-    def coords(p):
-        return {"sp": (base + p) // count_dp, "dp": lax.rem(base + p, count_dp)}
+    side = z // 2
+    inside = (z * (LINE - 1 - z)) // 2
+    mate_z = z + 1 - 2 * lax.rem(z, 2)
+    near_z = 2 - side
+    last_z = 3 - 3 * side
+
+    def on_line(other):
+        return {"sp": other * inner + y}
+
+    def on_plane(p):
+        return {"sp": z * inner + p // count_dp, "dp": lax.rem(p, count_dp)}
 
     barrier = pltpu.get_barrier_semaphore()
 
     def greet(d, carry):
         pl.semaphore_signal(
-            barrier, inc=1, device_id=coords(lax.rem(me + d, half)), device_id_type=MESH
+            barrier, inc=1, device_id=on_plane(lax.rem(me + d, peers)), device_id_type=MESH
         )
         return carry
 
-    lax.fori_loop(1, half, greet, 0)
-    pl.semaphore_signal(barrier, inc=1, device_id=partner, device_id_type=MESH)
-
-    def rows_of(b, i):
-        return pl.ds(pl.multiple_of((b * half + i) * capacity, capacity), capacity)
+    lax.fori_loop(1, peers, greet, 0)
+    for other in (mate_z, near_z, last_z):
+        pl.semaphore_signal(barrier, inc=1, device_id=on_line(other), device_id_type=MESH)
+
+    def rows_of(i):
+        return pl.ds(pl.multiple_of(i * capacity, capacity), capacity)
 
     def part(c):
         return pl.ds(c * span, span)
 
     def offset(i):
-        return 1 + lax.rem(i + half // 2 - 2, half - 1)
-
-    def to_partner(src, dst, sent, got):
+        return 1 + lax.rem(i + peers // 2 - 2, peers - 1)
+
+    def to_line(src, dst, sent, got, other):
         return pltpu.make_async_remote_copy(
             src_ref=src,
             dst_ref=dst,
             send_sem=sent,
             recv_sem=got,
-            device_id=partner,
+            device_id=on_line(other),
             device_id_type=MESH,
         )
 
-    far = [
-        to_partner(xin_ref.at[:, part(c)], xin_far.at[:, part(c)], far_send.at[c], far_recv.at[c])
-        for c in range(PARTS)
-    ]
-    far.append(to_partner(routes_ref, routes_far, far_send.at[PARTS], far_recv.at[PARTS]))
-    far.append(
-        to_partner(weights_ref, weights_far, far_send.at[PARTS + 1], far_recv.at[PARTS + 1])
-    )
-    far_back = [
-        to_partner(partial.at[:, part(c)], far_sum.at[:, part(c)], sum_send.at[c], sum_recv.at[c])
-        for c in range(PARTS)
-    ]
-
-    def outgoing(b, c, i):
-        p = lax.rem(me + offset(i), half)
+    tables = []
+    for k, (other, slot) in enumerate(((mate_z, 0), (near_z, 2 - inside), (last_z, 2 - inside))):
+        for t, (src, dst) in enumerate(((routes_ref, routes_far), (weights_ref, weights_far))):
+            tables.append(
+                to_line(src, dst.at[slot], table_send.at[k, t], table_recv.at[slot, t], other)
+            )
+
+    def tables_here(s):
+        for t, (src, dst) in enumerate(((routes_ref, routes_far), (weights_ref, weights_far))):
+            to_line(
+                src, dst.at[s - 1], table_send.at[0, t], table_recv.at[s - 1, t], mate_z
+            ).wait_recv()
+
+    def to_mate(c):
+        return to_line(
+            xin_ref.at[:, part(c)],
+            xin_far.at[0, :, part(c)],
+            line_send.at[0, c],
+            line_recv.at[0, c],
+            mate_z,
+        )
+
+    def to_near(c):
+        slot = 2 - inside
+        return to_line(
+            xin_ref.at[:, part(c)],
+            xin_far.at[slot, :, part(c)],
+            line_send.at[1, c],
+            line_recv.at[slot, c],
+            near_z,
+        )
+
+    def relay(s, c):
+        held = xin_far.at[s - 1, :, part(c)]
+        return to_line(held, held, line_send.at[s, c], line_recv.at[s - 1, c], mate_z)
+
+    def line_here(s, c):
+        held = xin_far.at[s - 1, :, part(c)]
+        to_line(held, held, line_send.at[0, c], line_recv.at[s - 1, c], mate_z).wait_recv()
+
+    def sum_out(s, c):
+        if s == 1:
+            other, slot = mate_z, 0
+        else:
+            beyond = near_z if s == 2 else last_z
+            other = inside * beyond + (1 - inside) * mate_z
+            slot = inside + (1 - inside) * s
+        return to_line(
+            partial.at[s - 1, :, part(c)],
+            inbox.at[slot, :, part(c)],
+            sum_send.at[s - 1, c],
+            sum_recv.at[slot, c],
+            other,
+        )
+
+    def sum_here(slot, c):
+        held = inbox.at[slot, :, part(c)]
+        to_line(held, held, sum_send.at[0, c], sum_recv.at[slot, c], mate_z).wait_recv()
+
+    def outgoing(s, c, i):
+        p = lax.rem(me + offset(i), peers)
         return pltpu.make_async_remote_copy(
-            src_ref=buffer.at[rows_of(b, p), part(c)],
-            dst_ref=received.at[rows_of(b, i), part(c)],
-            send_sem=send_sem.at[b, c, i],
-            recv_sem=recv_sem.at[b, c, i],
-            device_id=coords(p),
+            src_ref=buffer.at[s, rows_of(p), part(c)],
+            dst_ref=received.at[s, rows_of(i), part(c)],
+            send_sem=send_sem.at[s, c, i],
+            recv_sem=recv_sem.at[s, c, i],
+            device_id=on_plane(p),
             device_id_type=MESH,
         )
 
-    def returning(b, c, i):
-        p = lax.rem(me + half - offset(i), half)
+    def returning(s, c, i):
+        p = lax.rem(me + peers - offset(i), peers)
         return pltpu.make_async_remote_copy(
-            src_ref=results.at[rows_of(b, i), part(c)],
-            dst_ref=returned.at[rows_of(b, me), part(c)],
-            send_sem=back_send.at[b, c, i],
-            recv_sem=back_recv.at[b, c, i],
-            device_id=coords(p),
+            src_ref=results.at[s, rows_of(i), part(c)],
+            dst_ref=returned.at[s, rows_of(me), part(c)],
+            send_sem=back_send.at[s, c, i],
+            recv_sem=back_recv.at[s, c, i],
+            device_id=on_plane(p),
             device_id_type=MESH,
         )
 
-    def own_in(b, c):
+    def own_in(s, c):
         return pltpu.make_async_copy(
-            buffer.at[rows_of(b, me), part(c)],
-            received.at[rows_of(b, 0), part(c)],
-            own_sem.at[0, b, c],
-        )
-
-    def own_out(b, c):
+            buffer.at[s, rows_of(me), part(c)],
+            received.at[s, rows_of(0), part(c)],
+            own_sem.at[0, s, c],
+        )
+
+    def own_out(s, c):
         return pltpu.make_async_copy(
-            results.at[rows_of(b, 0), part(c)],
-            returned.at[rows_of(b, me), part(c)],
-            own_sem.at[1, b, c],
+            results.at[s, rows_of(0), part(c)],
+            returned.at[s, rows_of(me), part(c)],
+            own_sem.at[1, s, c],
         )
 
     loads = [
         pltpu.make_async_copy(src, dst, weight_sem.at[j])
         for j, (src, dst) in enumerate(((gate_hbm, gate), (up_hbm, up), (down_hbm, down)))
     ]
+    for load in loads:
+        load.start()
 
     def each(do):
         def body(i, carry):
             do(i)
             return carry
 
-        lax.fori_loop(1, half, body, 0)
-
-    pl.semaphore_wait(barrier, half)
-    far[PARTS].start()
-    far[PARTS + 1].start()
+        lax.fori_loop(1, peers, body, 0)
+
+    pl.semaphore_wait(barrier, peers + 2)
+    for copy in tables:
+        copy.start()
     for c in range(PARTS):
-        far[c].start()
-
-    def spread(b, c, masks, source):
-        picks = jnp.where(masks[0] | masks[1], 1.0, 0.0).astype(jnp.bfloat16)
-        block = slice(b * half * capacity, (b + 1) * half * capacity)
-        buffer[block, c * span : (c + 1) * span] = jnp.dot(
-            picks, source[:, c * span : (c + 1) * span], preferred_element_type=jnp.float32
-        ).astype(jnp.bfloat16)
-        each(lambda i: outgoing(b, c, i).start())
-        own_in(b, c).start()
-
-    def combines(masks, weights):
+        to_mate(c).start()
+    for c in range(PARTS):
+        to_near(c).start()
+
+    first_expert = z * peers
+
+    def masks_of(s):
+        routes = routes_ref[...] if s == 0 else routes_far[s - 1]
+        return slot_masks(routes, first_expert, count, peers, capacity)
+
+    def picks_of(masks):
+        return jnp.where(masks[0] | masks[1], 1.0, 0.0).astype(jnp.bfloat16)
+
+    def combines(s, masks):
+        weights = weights_ref[...] if s == 0 else weights_far[s - 1]
         combine = (
             jnp.where(masks[0], weights[0:1, :], 0.0) + jnp.where(masks[1], weights[1:2, :], 0.0)
         ).T
         high = combine.astype(jnp.bfloat16)
         return high, (combine - high.astype(jnp.float32)).astype(jnp.bfloat16)
 
-    def combined(pair, b, c):
-        block = returned[
-            b * half * capacity : (b + 1) * half * capacity, c * span : (c + 1) * span
-        ]
+    def spread(s, c, picks):
+        cols = slice(c * span, (c + 1) * span)
+        source = xin_ref[:, cols] if s == 0 else xin_far[s - 1, :, cols]
+        buffer[s, :, cols] = jnp.dot(picks, source, preferred_element_type=jnp.float32).astype(
+            jnp.bfloat16
+        )
+        each(lambda i: outgoing(s, c, i).start())
+        own_in(s, c).start()
+
+    def combined(s, c, pair):
+        block = returned[s, :, c * span : (c + 1) * span]
         return jnp.dot(pair[0], block, preferred_element_type=jnp.float32) + jnp.dot(
             pair[1], block, preferred_element_type=jnp.float32
         )
 
-    near_masks = slot_masks(routes_ref[...], base, count, half, capacity)
+    def compute(s):
+        for c in range(PARTS):
+            own_in(s, c).wait()
+            each(lambda i, c=c: outgoing(s, c, i).wait_recv())
+
+        def make_hidden(j, carry):
+            cols = pl.ds(pl.multiple_of(j * 256, 256), 256)
+            gate_part = jnp.dot(received[s], gate[:, cols], preferred_element_type=jnp.float32)
+            up_part = jnp.dot(received[s], up[:, cols], preferred_element_type=jnp.float32)
+            hidden[:, cols] = (jax.nn.silu(gate_part) * up_part).astype(jnp.bfloat16)
+            return carry
+
+        lax.fori_loop(0, width // 256, make_hidden, 0)
+        for c in range(PARTS):
+            cols = slice(c * span, (c + 1) * span)
+            results[s, :, cols] = jnp.dot(
+                hidden[...], down[:, cols], preferred_element_type=jnp.float32
+            ).astype(jnp.bfloat16)
+            own_out(s, c).start()
+            each(lambda i, c=c: returning(s, c, i).start())
+
+    def returned_here(s, c):
+        own_out(s, c).wait()
+        each(lambda i: returning(s, c, i).wait_recv())
+
+    def send_sums(s, pair):
+        for c in range(PARTS):
+            cols = slice(c * span, (c + 1) * span)
+            returned_here(s, c)
+            total = combined(s, c, pair)
+            if s == 1:
+                partial[s - 1, :, cols] = total.astype(jnp.bfloat16)
+            else:
+
+                @pl.when(inside == 0)
+                def _(total=total, cols=cols):
+                    partial[s - 1, :, cols] = total.astype(jnp.bfloat16)
+
+                @pl.when(inside == 1)
+                def _(total=total, cols=cols, c=c):
+                    sum_here(s, c)
+                    partial[s - 1, :, cols] = (
+                        total + inbox[s, :, cols].astype(jnp.float32)
+                    ).astype(jnp.bfloat16)
+
+            sum_out(s, c).start()
+
+    def relays(s):
+        @pl.when(inside == 1)
+        def _():
+            for c in range(PARTS):
+                line_here(s, c)
+                relay(s, c).start()
+
+    def dispatch(s, picks):
+        for c in range(PARTS):
+            if s in (2, 3):
+
+                @pl.when(inside == 0)
+                def _(c=c):
+                    line_here(s, c)
+            else:
+                line_here(s, c)
+            spread(s, c, picks)
+
+    masks = masks_of(0)
+    picks = picks_of(masks)
     for c in range(PARTS):
-        spread(0, c, near_masks, xin_ref)
-    for load in loads:
-        load.start()
-    near_pair = combines(near_masks, weights_ref[...])
-
-    far[PARTS].wait_recv()
-    far[PARTS + 1].wait_recv()
-    far_masks = slot_masks(routes_far[...], base, count, half, capacity)
-    far_pair = combines(far_masks, weights_far[...])
-    for c in range(PARTS):
-        far[c].wait_recv()
-        spread(1, c, far_masks, xin_far)
+        spread(0, c, picks)
+    pairs = [combines(0, masks)]
+    later = []
+    for s in (1, 2, 3):
+        tables_here(s)
+        masks = masks_of(s)
+        later.append(picks_of(masks))
+        pairs.append(combines(s, masks))
     for load in loads:
         load.wait()
 
-    for b in range(2):
-        at = slice(b * half * capacity, (b + 1) * half * capacity)
+    compute(0)
+    relays(2)
+    dispatch(1, later[0])
+    compute(1)
+    relays(3)
+    dispatch(2, later[1])
+    send_sums(1, pairs[1])
+    compute(2)
+    dispatch(3, later[2])
+    send_sums(2, pairs[2])
+    compute(3)
+    for c in range(PARTS):
+        cols = slice(c * span, (c + 1) * span)
+        returned_here(0, c)
+        sum_here(0, c)
+        near_sum[:, cols] = (
+            mid_ref[:, cols].astype(jnp.float32)
+            + combined(0, c, pairs[0])
+            + inbox[0, :, cols].astype(jnp.float32)
+        )
+    send_sums(3, pairs[3])
+    for c in range(PARTS):
+        cols = slice(c * span, (c + 1) * span)
+        sum_here(1, c)
+        out_ref[:, cols] = (near_sum[:, cols] + inbox[1, :, cols].astype(jnp.float32)).astype(
+            jnp.bfloat16
+        )
+
+    for copy in tables:
+        copy.wait_send()
+    for c in range(PARTS):
+        to_mate(c).wait_send()
+        to_near(c).wait_send()
+        for s in (1, 2, 3):
+            sum_out(s, c).wait_send()
+
+    @pl.when(inside == 1)
+    def _():
         for c in range(PARTS):
-            own_in(b, c).wait()
-            each(lambda i, b=b, c=c: outgoing(b, c, i).wait_recv())
-
-        def make_hidden(j, carry, at=at):
-            cols = pl.ds(pl.multiple_of(j * 256, 256), 256)
-            gate_part = jnp.dot(received[at, :], gate[:, cols], preferred_element_type=jnp.float32)
-            up_part = jnp.dot(received[at, :], up[:, cols], preferred_element_type=jnp.float32)
-            hidden[:, cols] = (jax.nn.silu(gate_part) * up_part).astype(jnp.bfloat16)
-            return carry
-
-        lax.fori_loop(0, width // 256, make_hidden, 0)
-        for c in range(PARTS):
-
-            def make_out(j, carry, at=at, c=c):
-                cols = pl.ds(pl.multiple_of(c * span + j * 512, 512), 512)
-                results[at, cols] = jnp.dot(
-                    hidden[...], down[:, cols], preferred_element_type=jnp.float32
-                ).astype(jnp.bfloat16)
-                return carry
-
-            lax.fori_loop(0, span // 512, make_out, 0)
-            if b == 1:
-                each(lambda i, c=c: returning(1, c, i).start())
-    for b in (1, 0):
-        for c in range(PARTS):
-            own_out(b, c).start()
-    for c in range(PARTS):
-        each(lambda i, c=c: returning(0, c, i).start())
-
-    for c in range(PARTS):
-        own_out(1, c).wait()
-        each(lambda i, c=c: returning(1, c, i).wait_recv())
-        partial[:, c * span : (c + 1) * span] = combined(far_pair, 1, c).astype(jnp.bfloat16)
-        far_back[c].start()
-    for c in range(PARTS):
-        own_out(0, c).wait()
-        each(lambda i, c=c: returning(0, c, i).wait_recv())
-        near = combined(near_pair, 0, c)
-        far_back[c].wait_recv()
-        cols = slice(c * span, (c + 1) * span)
-        out_ref[:, cols] = (
-            mid_ref[:, cols].astype(jnp.float32) + near + far_sum[:, cols].astype(jnp.float32)
-        ).astype(jnp.bfloat16)
-
-    for copy in far + far_back:
-        copy.wait_send()
+            relay(2, c).wait_send()
+            relay(3, c).wait_send()
 
     def drain(i):
-        for b in range(2):
+        for s in range(LINE):
             for c in range(PARTS):
-                outgoing(b, c, i).wait_send()
-                returning(b, c, i).wait_send()
+                outgoing(s, c, i).wait_send()
+                returning(s, c, i).wait_send()
 
     each(drain)
 
@@ -577,7 +702,7 @@
     experts_all = count_sp * count_dp
     rows = residual.shape[1]
     capacity = max(2, 4 * rows // experts_all)
-    if capacity % 16 or count_sp % 2:
+    if capacity % 16 or count_sp % LINE:
         return on_device(
             residual,
             query_maps,
@@ -594,7 +719,8 @@
             expert_down,
         )
     heads_here = HEADS // count_sp
-    slots = experts_all * capacity
+    peers = experts_all // LINE
+    slots = peers * capacity
     vmem = pl.BlockSpec(memory_space=pltpu.VMEM)
     hbm = pl.BlockSpec(memory_space=pl.ANY)
     dma = pltpu.SemaphoreType.DMA
@@ -642,28 +768,31 @@
         in_specs=[vmem, vmem, vmem, vmem, hbm, hbm, hbm],
         out_specs=vmem,
         scratch_shapes=[
-            pltpu.VMEM((routes.shape[2], rows), jnp.int32),
-            pltpu.VMEM((routes.shape[2], rows), jnp.float32),
-            pltpu.VMEM((rows, D), bf16),
-            pltpu.VMEM((rows, D), bf16),
-            pltpu.VMEM((rows, D), bf16),
-            pltpu.VMEM((slots, D), bf16),
-            pltpu.VMEM((slots, D), bf16),
-            pltpu.VMEM((slots, D), bf16),
-            pltpu.VMEM((slots, D), bf16),
+            pltpu.VMEM((LINE - 1, routes.shape[2], rows), jnp.int32),
+            pltpu.VMEM((LINE - 1, routes.shape[2], rows), jnp.float32),
+            pltpu.VMEM((LINE - 1, rows, D), bf16),
+            pltpu.VMEM((LINE - 1, rows, D), bf16),
+            pltpu.VMEM((LINE, rows, D), bf16),
+            pltpu.VMEM((rows, D), jnp.float32),
+            pltpu.VMEM((LINE, slots, D), bf16),
+            pltpu.VMEM((LINE, slots, D), bf16),
+            pltpu.VMEM((LINE, slots, D), bf16),
+            pltpu.VMEM((LINE, slots, D), bf16),
             pltpu.VMEM((D, width), bf16),
             pltpu.VMEM((D, width), bf16),
             pltpu.VMEM((width, D), bf16),
-            pltpu.VMEM((slots // 2, width), bf16),
-            dma((PARTS + 2,)),
-            dma((PARTS + 2,)),
-            dma((PARTS,)),
-            dma((PARTS,)),
-            dma((2, PARTS, experts_all // 2)),
-            dma((2, PARTS, experts_all // 2)),
-            dma((2, PARTS, experts_all // 2)),
-            dma((2, PARTS, experts_all // 2)),
-            dma((2, 2, PARTS)),
+            pltpu.VMEM((slots, width), bf16),
+            dma((LINE - 1, 2)),
+            dma((LINE - 1, 2)),
+            dma((LINE, PARTS)),
+            dma((LINE - 1, PARTS)),
+            dma((LINE - 1, PARTS)),
+            dma((LINE, PARTS)),
+            dma((LINE, PARTS, peers)),
+            dma((LINE, PARTS, peers)),
+            dma((LINE, PARTS, peers)),
+            dma((LINE, PARTS, peers)),
+            dma((2, LINE, PARTS)),
             dma((3,)),
         ],
         compiler_params=pltpu.CompilerParams(

time: 144 us -> 150 us (1.042)
  Pallas kernels: 142 us -> 148 us
    pallas_call x1, Pallas kernels: 85.4 us -> 91.2 us  [kernels_on_device(): pl.pallas_call(functools.partial(experts_kernel, count_sp, count_dp, capa...]
where the time goes in v1:
time: 150 us
  Pallas kernels  148 us (99%)
  local copies, waits for them, and re-layouts  1.88 us (1%)
    pallas_call x1, Pallas kernels, kernels_on_device(): pl.pallas_call(functools.partial(experts_kernel, count_sp, count_dp, capa...  91.2 us
    pallas_call x1, Pallas kernels, kernels_on_device(): pl.pallas_call(functools.partial(mixer_kernel, count_sp), out_shape=(jax....  56.5 us

profile of v1, /device:TPU:0, one launch (start us, length us, event | category | flops | bytes accessed | tf_op | source)
XLA Modules:
  0.0 149.6 jit_solution(8152836448079985132)
XLA Ops:
  0.0 56.5 %shard_map.127 = (bf16[128,2048]{1,0:T(8,128)(2,1)}, bf16[128,2048]{1,0:T(8,128)(2,1)}) custom-call(f32[16]{0:T(128)} %lam_ref.1, bf16[128,2048]{1,0:T(8,128)(2,1)} %bitcast.20, bf16[128,2048]{1,0:T(8,128)(2,1)} %bitcast.21, bf16[128,2048]{1,0:T(8,128)(2,1)} %bitcast.22, bf16[128,2048]{1,0:T(8,128)(2,1)} %bitcast.23, f32[16,128]{1,0:T(8,128)} %bitcast.24, ...), custom_call_target="tpu_custom_call" | custom-call | tf_op jit(solution)/shard_map/pallas_call | solution.py:729
  56.5 91.2 %shard_map.128 = bf16[128,2048]{1,0:T(8,128)(2,1)} custom-call(bf16[128,2048]{1,0:T(8,128)(2,1)} %get-tuple-element.7.xin_ref, bf16[128,2048]{1,0:T(8,128)(2,1)} %get-tuple-element.8.mid_ref, s32[2,128]{1,0:T(2,128)} %bitcast.26, f32[2,128]{1,0:T(2,128)} %bitcast.27, bf16[2048,1024]{1,0:T(8,128)(2,1)} %bitcast.16, bf16[2048,1024]{1,0:T(8,128)(2,1)} %bitcast.17, ...), custom_call_target="tpu_custom_call" | custom-call | tf_op jit(solution)/shard_map/pallas_call | solution.py:765
  147.8 1.9 %copy.15 = bf16[1,128,2048]{2,1,0:T(8,128)(2,1)} copy(bf16[1,128,2048]{2,1,0:T(8,128)(2,1)} %bitcast.19) | data formatting | bytes 1048576

commit v2 on v0

v2 whole, which is shorter than its diff:
```python
import functools
import math

import jax
import jax.numpy as jnp
from jax import lax
from jax.experimental import pallas as pl
from jax.experimental.pallas import tpu as pltpu
from jax.sharding import PartitionSpec as P

D = 2048
HEADS = 16
HD = 64
VD = 128


eps = 1e-06


def attend_head(query_head, key_head, value_head, lam_head, gain_head):
    length = query_head.shape[0]
    block_rows = min(512, length)
    count_blocks = length // block_rows
    scaling = query_head.shape[-1] ** (-0.5)
    query_blocks = query_head.reshape(count_blocks, block_rows, 2, query_head.shape[-1])

    def one_block(query_block):
        scores = (
            jnp.einsum("qmd,kmd->mqk", query_block, key_head, preferred_element_type=jnp.float32)
            * scaling
        )
        probabilities = jax.nn.softmax(scores, axis=-1)
        mixed_map = (probabilities[0] - lam_head * probabilities[1]).astype(jnp.bfloat16)
        head_out = jnp.dot(mixed_map, value_head, preferred_element_type=jnp.float32)
        normed = head_out * lax.rsqrt(jnp.mean(head_out * head_out, axis=-1, keepdims=True) + eps)
        return (normed * gain_head * 0.8).astype(jnp.bfloat16)

    return lax.map(one_block, query_blocks).reshape(length, value_head.shape[-1])


def on_device(
    residual,
    query_maps,
    key_maps,
    value_rows,
    lambdas,
    head_gain,
    out_weight,
    ffn_gain,
    routes,
    route_weights,
    expert_gate,
    expert_up,
    expert_down,
):
    count_sp = lax.axis_size("sp")
    count_dp = lax.axis_size("dp")
    heads_here = HEADS // count_sp
    queries, keys_all, values_all = (
        lax.all_to_all(query_maps, "sp", split_axis=2, concat_axis=1, tiled=True),
        lax.all_to_all(key_maps, "sp", split_axis=2, concat_axis=1, tiled=True),
        lax.all_to_all(value_rows, "sp", split_axis=2, concat_axis=1, tiled=True),
    )
    first_head = lax.axis_index("sp") * heads_here
    lam_here = lax.dynamic_slice_in_dim(lambdas, first_head, heads_here)
    gain_here = lax.dynamic_slice_in_dim(head_gain, first_head * VD, heads_here * VD)
    outputs = []
    for head_index in range(heads_here):
        query_head = queries[0, :, head_index * 2 * HD : (head_index + 1) * 2 * HD].reshape(
            -1, 2, HD
        )
        key_head = keys_all[0, :, head_index * 2 * HD : (head_index + 1) * 2 * HD].reshape(
            -1, 2, HD
        )
        value_head = values_all[0, :, head_index * VD : (head_index + 1) * VD]
        gain_head = gain_here[head_index * VD : (head_index + 1) * VD]
        outputs.append(
            attend_head(query_head, key_head, value_head, lam_here[head_index], gain_head)
        )
    attended = jnp.concatenate(outputs, axis=1)[None]
    returned_heads = lax.all_to_all(attended, "sp", split_axis=1, concat_axis=2, tiled=True)
    projected = jnp.dot(returned_heads[0], out_weight, preferred_element_type=jnp.float32)
    residual_mid = (residual[0].astype(jnp.float32) + projected).astype(jnp.bfloat16)
    middle = residual_mid.astype(jnp.float32)
    expert_input = (
        middle * lax.rsqrt(jnp.mean(middle * middle, axis=-1, keepdims=True) + eps) * ffn_gain
    ).astype(jnp.bfloat16)
    tok_rows = residual.shape[1]
    experts_all = count_sp * count_dp
    capacity = max(2, 4 * tok_rows // experts_all)
    flat_routes = routes[0].reshape(-1)
    flat_weights = route_weights[0].reshape(-1)
    onehot = (flat_routes[:, None] == jnp.arange(experts_all, dtype=jnp.int32)[None, :]).astype(
        jnp.int32
    )
    before = jnp.cumsum(onehot, axis=0) - onehot
    rank_of = jnp.sum(before * onehot, axis=1)
    slot = flat_routes * capacity + rank_of
    token_of = jnp.arange(flat_routes.shape[0], dtype=jnp.int32) // routes.shape[2]
    slot_token = jnp.full((experts_all * capacity,), tok_rows, jnp.int32).at[slot].set(token_of)
    padded_input = jnp.concatenate([expert_input, jnp.zeros((1, D), jnp.bfloat16)], axis=0)
    buffer = padded_input[slot_token].reshape(experts_all, capacity, D)
    received = lax.all_to_all(buffer, ("sp", "dp"), split_axis=0, concat_axis=0, tiled=True)
    row_block = received.reshape(-1, D)
    gate_part = jnp.dot(row_block, expert_gate[0], preferred_element_type=jnp.float32)
    up_part = jnp.dot(row_block, expert_up[0], preferred_element_type=jnp.float32)
    hidden = (jax.nn.silu(gate_part) * up_part).astype(jnp.bfloat16)
    expert_out = jnp.dot(hidden, expert_down[0], preferred_element_type=jnp.float32).astype(
        jnp.bfloat16
    )
    returned = lax.all_to_all(
        expert_out.reshape(received.shape), ("sp", "dp"), split_axis=0, concat_axis=0, tiled=True
    )
    picked = returned.reshape(experts_all * capacity, D)[slot]
    weighted = (picked.astype(jnp.float32) * flat_weights[:, None]).reshape(
        tok_rows, routes.shape[2], D
    )
    layer_out = (middle + jnp.sum(weighted, axis=1)).astype(jnp.bfloat16)
    return layer_out[None]


MESH = pl.DeviceIdType.MESH
VMEM_LIMIT = 60 * 1024 * 1024


def slot_masks(routes, first_expert, experts_all, experts_here, capacity):
    rows = routes.shape[1]
    first, second = routes[0:1, :], routes[1:2, :]
    experts = lax.broadcasted_iota(jnp.int32, (experts_all, rows), 0)
    named_first, named_second = experts == first, experts == second
    named = jnp.where(named_first | named_second, 1.0, 0.0).astype(jnp.bfloat16)
    earlier = lax.broadcasted_iota(jnp.int32, (rows, rows), 0) < lax.broadcasted_iota(
        jnp.int32, (rows, rows), 1
    )
    before = jnp.dot(
        named, jnp.where(earlier, 1.0, 0.0).astype(jnp.bfloat16), preferred_element_type=jnp.float32
    )
    slots = lax.broadcasted_iota(jnp.int32, (experts_here * capacity, rows), 0)
    masks = []
    for route, chosen in ((first, named_first), (second, named_second)):
        rank = jnp.sum(jnp.where(chosen, before, 0.0), axis=0, keepdims=True).astype(jnp.int32)
        masks.append(slots == (route - first_expert) * capacity + rank)
    return masks


PARTS = 4
LINE = 4


def layer_kernel(
    count_sp,
    count_dp,
    capacity,
    lam_ref,
    q_ref,
    k_ref,
    v_ref,
    residual_ref,
    gain_ref,
    ow_hbm,
    fgain_ref,
    routes_ref,
    weights_ref,
    gate_hbm,
    up_hbm,
    down_hbm,
    out_ref,
    staged,
    qh,
    kh,
    vh,
    outs,
    att,
    ow,
    mid,
    xin,
    routes_far,
    weights_far,
    picks,
    shares,
    far,
    partial,
    inbox,
    total,
    buffer,
    received,
    results,
    returned,
    far_buffer,
    far_received,
    far_results,
    far_returned,
    gate,
    up,
    down,
    hidden,
    send_sem,
    key_recv,
    query_recv,
    value_recv,
    back_send,
    back_recv,
    ow_sem,
    weight_sem,
    table_send,
    table_recv,
    far_send,
    far_recv,
    relay_send,
    sum_send,
    sum_recv,
    go_send,
    go_recv,
    ret_send,
    ret_recv,
    fgo_send,
    fgo_recv,
    fret_send,
    fret_recv,
    stage_sem,
):
    me_sp = lax.axis_index("sp")
    rows = q_ref.shape[0]
    heads_here = HEADS // count_sp
    sources = ((staged.at[0], kh), (staged.at[1], qh), (staged.at[2], vh))
    stages = [
        pltpu.make_async_copy(src, staged.at[t], stage_sem.at[t])
        for t, src in enumerate((k_ref, q_ref, v_ref))
    ]
    for t in (0, 2, 1):
        stages[t].start()

    count = count_sp * count_dp
    inner = count_sp // LINE
    half = count // 2
    plane = half // 2
    z, y = me_sp // inner, lax.rem(me_sp, inner)
    side = z // 2
    base = side * half
    me = me_sp * count_dp + lax.axis_index("dp") - base
    me_z, me_j = me // plane, lax.rem(me, plane)
    inside = (z * (LINE - 1 - z)) // 2
    gate_z = 1 - side
    mate_z = z + 1 - 2 * lax.rem(z, 2)
    near_z = 2 - side
    last_z = 3 - 3 * side
    width = gate.shape[1]
    span = D // PARTS

    def coords(p):
        return {"sp": (base + p) // count_dp, "dp": lax.rem(base + p, count_dp)}

    def on_line(other):
        return {"sp": other * inner + y}

    def peer(i):
        e = i + i // plane
        return lax.rem(me_z + 1 + e // plane, 2) * plane + lax.rem(me_j + e, plane)

    barrier = pltpu.get_barrier_semaphore()

    def greet(d, carry):
        pl.semaphore_signal(
            barrier, inc=1, device_id={"sp": lax.rem(me_sp + d, count_sp)}, device_id_type=MESH
        )
        return carry

    lax.fori_loop(1, count_sp, greet, 0)

    def greet_half(i, carry):
        pl.semaphore_signal(barrier, inc=1, device_id=coords(peer(i)), device_id_type=MESH)
        return carry

    lax.fori_loop(0, half - 1, greet_half, 0)

    my_rows = pl.ds(pl.multiple_of(me_sp * rows, rows), rows)

    def arrival(t, h, d):
        return (key_recv.at[h], query_recv.at[h, d], value_recv.at[h])[t]

    def local_copy(t, h):
        src, dst = sources[t]
        cols = pl.ds(pl.multiple_of((me_sp * heads_here + h) * VD, VD), VD)
        return pltpu.make_async_copy(src.at[:, cols], dst.at[h, my_rows, :], arrival(t, h, 0))

    def outgoing(t, h, d):
        src, dst = sources[t]
        to = lax.rem(me_sp + d, count_sp)
        cols = pl.ds(pl.multiple_of((to * heads_here + h) * VD, VD), VD)
        return pltpu.make_async_remote_copy(
            src_ref=src.at[:, cols],
            dst_ref=dst.at[h, my_rows, :],
            send_sem=send_sem,
            recv_sem=arrival(t, h, d),
            device_id={"sp": to},
            device_id_type=MESH,
        )

    def landed(ref, sem):
        pltpu.make_async_copy(ref, ref, sem).wait()

    def table(t, n, slot):
        src, dst = ((routes_ref, routes_far), (weights_ref, weights_far))[t]
        return pltpu.make_async_remote_copy(
            src_ref=src,
            dst_ref=dst.at[slot],
            send_sem=table_send.at[t, n],
            recv_sem=table_recv.at[slot, t],
            device_id=on_line((near_z, last_z)[n]),
            device_id_type=MESH,
        )

    weight_copy = pltpu.make_async_copy(ow_hbm, ow, ow_sem)
    loads = [
        pltpu.make_async_copy(src, dst, weight_sem.at[j])
        for j, (src, dst) in enumerate(((gate_hbm, gate), (up_hbm, up), (down_hbm, down)))
    ]

    pl.semaphore_wait(barrier, count_sp - 1 + half - 1)
    for h in range(heads_here):

        for t in (0, 2, 1):
            if h == 0:
                stages[t].wait()

            def start_all(i, carry, t=t, h=h):
                outgoing(t, h, 1 + lax.rem(i + count_sp // 2 - 1, count_sp - 1)).start()
                return carry

            lax.fori_loop(0, count_sp - 1, start_all, 0)
            local_copy(t, h).start()
    for n in range(2):
        for t in range(2):
            table(t, n, 1 - inside).start()
    weight_copy.start()
    for load in loads:
        load.start()

    def set_tables(slot, routes, weights):
        masks = slot_masks(routes, base, count, half, capacity)
        picks[slot] = jnp.where(masks[0] | masks[1], 1.0, 0.0).astype(jnp.bfloat16)
        combine = (
            jnp.where(masks[0], weights[0:1, :], 0.0) + jnp.where(masks[1], weights[1:2, :], 0.0)
        ).T
        high = combine.astype(jnp.bfloat16)
        shares[slot, 0] = high
        shares[slot, 1] = (combine - high.astype(jnp.float32)).astype(jnp.bfloat16)

    set_tables(0, routes_ref[...], weights_ref[...])

    def returning(h, p, d):
        dst_cols = pl.ds(pl.multiple_of((me_sp * heads_here + h) * VD, VD), VD)
        return pltpu.make_async_remote_copy(
            src_ref=outs.at[h, pl.ds(pl.multiple_of(p * rows, rows), rows), :],
            dst_ref=att.at[:, dst_cols],
            send_sem=back_send,
            recv_sem=back_recv,
            device_id={"sp": p},
            device_id_type=MESH,
        )

    factor = HD ** (-0.5) * math.log2(math.e)
    lanes = lax.broadcasted_iota(jnp.int32, (rows, VD), 1)
    for h in range(heads_here):
        with jax.named_scope("kv"):
            landed(kh.at[h], key_recv.at[h])
            landed(vh.at[h], value_recv.at[h])
        head = me_sp * heads_here + h
        lam = lam_ref[head]
        gain = gain_ref[pl.ds(head, 1), :]

        def attend(p, h=h, lam=lam, gain=gain):
            at = pl.ds(pl.multiple_of(p * rows, rows), rows)
            q = qh[h, at, :]
            zero = jnp.zeros_like(q)
            both = jnp.concatenate(
                [jnp.where(lanes < HD, q, zero), jnp.where(lanes < HD, zero, q)], axis=0
            )
            scores = lax.dot_general(
                both, kh[h], (((1,), (1,)), ((), ())), preferred_element_type=jnp.float32
            )
            top = jnp.max(scores, axis=1, keepdims=True)
            e = jnp.exp2((scores - top) * factor)
            norm = jnp.sum(e, axis=1, keepdims=True)
            norm_1, norm_2 = norm[:rows], norm[rows:]
            share = lam * norm_1 / norm_2
            mixed = (e[:rows] - share * e[rows:]).astype(jnp.bfloat16)
            head_out = jnp.dot(mixed, vh[h], preferred_element_type=jnp.float32) / norm_1
            normed = head_out * lax.rsqrt(
                jnp.mean(head_out * head_out, axis=-1, keepdims=True) + eps
            )
            return (normed * gain * 0.8).astype(jnp.bfloat16)

        def step(i, carry, h=h, attend=attend):
            d = 1 + lax.rem(i + count_sp // 2 - 1, count_sp - 1)
            p = lax.rem(me_sp + count_sp - d, count_sp)
            outgoing(1, h, d).wait_recv()
            outs[h, pl.ds(pl.multiple_of(p * rows, rows), rows), :] = attend(p)
            returning(h, p, d).start()
            return carry

        with jax.named_scope("steps"):
            lax.fori_loop(0, count_sp - 1, step, 0)
        local_copy(1, h).wait()
        with jax.named_scope("mine"):
            att[:, pl.ds(pl.multiple_of(head * VD, VD), VD)] = attend(me_sp)

    for slot in range(2):
        for t in range(2):
            table(t, 0, slot).wait_recv()
        set_tables(1 + slot, routes_far[slot], weights_far[slot])

    weight_copy.wait()
    others = (count_sp - 1) * heads_here * VD
    with jax.named_scope("back"):
        landed(att.at[:, pl.ds(0, others)], back_recv)

    tile = 512
    square = jnp.zeros((rows, 1), jnp.float32)
    for j in range(D // tile):
        cols = slice(j * tile, (j + 1) * tile)
        projected = jnp.dot(att[...], ow[:, cols], preferred_element_type=jnp.float32)
        middle = (residual_ref[:, cols].astype(jnp.float32) + projected).astype(jnp.bfloat16)
        mid[:, cols] = middle
        wide = middle.astype(jnp.float32)
        square = square + jnp.sum(wide * wide, axis=1, keepdims=True)
    scale = lax.rsqrt(square / D + eps)
    xin[...] = (mid[...].astype(jnp.float32) * scale * fgain_ref[...]).astype(jnp.bfloat16)

    def rows_of(i):
        return pl.ds(pl.multiple_of(i * capacity, capacity), capacity)

    def part(c):
        return pl.ds(c * span, span)

    def remote(src, dst, sent, got, target):
        return pltpu.make_async_remote_copy(
            src_ref=src,
            dst_ref=dst,
            send_sem=sent,
            recv_sem=got,
            device_id=target,
            device_id_type=MESH,
        )

    def cross(c):
        slot = 1 - inside
        return remote(
            xin.at[:, part(c)],
            far.at[slot, :, part(c)],
            far_send,
            far_recv.at[slot, c],
            on_line(near_z),
        )

    def crossed(k, c):
        landed(far.at[k, :, part(c)], far_recv.at[k, c])

    def go(c, q, own):
        return remote(
            buffer.at[rows_of(q), part(c)],
            received.at[rows_of(me), part(c)],
            go_send,
            go_recv.at[own, c],
            coords(q),
        )

    def ret(c, q):
        return remote(
            results.at[rows_of(q), part(c)],
            returned.at[rows_of(me), part(c)],
            ret_send,
            ret_recv.at[c],
            coords(q),
        )

    def relay(k, c):
        held = far.at[k, :, part(c)]
        return remote(held, held, relay_send, far_recv.at[k, c], on_line(mate_z))

    def far_go(k, c, j):
        return remote(
            far_buffer.at[k, rows_of(j), part(c)],
            far_received.at[k, rows_of(me_j), part(c)],
            fgo_send,
            fgo_recv.at[k, c],
            coords(me_z * plane + j),
        )

    def far_ret(k, c, j):
        return remote(
            far_results.at[k, rows_of(j), part(c)],
            far_returned.at[k, rows_of(me), part(c)],
            fret_send,
            fret_recv.at[k, c],
            coords(gate_z * plane + j),
        )

    def sum_out(k, c):
        return remote(
            partial.at[k, :, part(c)],
            inbox.at[:, part(c)],
            sum_send,
            sum_recv.at[c],
            on_line(near_z if k == 0 else last_z),
        )

    def sum_here(c):
        landed(inbox.at[:, part(c)], sum_recv.at[c])

    def own_in(c):
        return pltpu.make_async_copy(
            buffer.at[rows_of(me), part(c)], received.at[rows_of(me), part(c)], go_recv.at[1, c]
        )

    def own_out(c):
        return pltpu.make_async_copy(
            results.at[rows_of(me), part(c)], returned.at[rows_of(me), part(c)], ret_recv.at[c]
        )

    def far_own_in(k, c):
        return pltpu.make_async_copy(
            far_buffer.at[k, rows_of(me_j), part(c)],
            far_received.at[k, rows_of(me_j), part(c)],
            fgo_recv.at[k, c],
        )

    def far_own_out(k, c):
        return pltpu.make_async_copy(
            far_results.at[k, rows_of(me_j), part(c)],
            far_returned.at[k, rows_of(me), part(c)],
            fret_recv.at[k, c],
        )

    def each(first, last, do):
        def loop(i, carry):
            do(i)
            return carry

        lax.fori_loop(first, last, loop, 0)

    def peers(do):
        each(0, half - 1, lambda i: do(peer(i)))

    def mates(do):
        each(1, plane, lambda i: do(lax.rem(me_j + i, plane)))

    def cut(c):
        return slice(c * span, (c + 1) * span)

    def spread(c):
        buffer[:, cut(c)] = jnp.dot(
            picks[0], xin[:, cut(c)], preferred_element_type=jnp.float32
        ).astype(jnp.bfloat16)
        mates(lambda j: go(c, me_z * plane + j, 1).start())
        own_in(c).start()

    def across(c):
        far_z = 1 - me_z
        each(0, plane, lambda i: go(c, far_z * plane + lax.rem(me_j + i, plane), 0).start())

    plane_rows = plane * capacity
    my_plane = pl.ds(pl.multiple_of(me_z * plane_rows, plane_rows), plane_rows)

    def far_spread(k, relaying):
        for c in range(PARTS):
            crossed(k, c)
            if relaying:
                relay(k, c).start()
            far_buffer[k, :, cut(c)] = jnp.dot(
                picks[1 + k, my_plane], far[k, :, cut(c)], preferred_element_type=jnp.float32
            ).astype(jnp.bfloat16)
            mates(lambda j, c=c: far_go(k, c, j).start())
            far_own_in(k, c).start()

    def expert(source, target, send):
        def make_hidden(j, carry):
            cols = pl.ds(pl.multiple_of(j * 256, 256), 256)
            gate_part = jnp.dot(source[...], gate[:, cols], preferred_element_type=jnp.float32)
            up_part = jnp.dot(source[...], up[:, cols], preferred_element_type=jnp.float32)
            hidden[:, cols] = (jax.nn.silu(gate_part) * up_part).astype(jnp.bfloat16)
            return carry

        lax.fori_loop(0, width // 256, make_hidden, 0)
        for c in range(PARTS):
            target[:, cut(c)] = jnp.dot(
                hidden[...], down[:, cut(c)], preferred_element_type=jnp.float32
            ).astype(jnp.bfloat16)
            send(c)

    def near_return(c, own):
        which = me_z if own else 1 - me_z
        if own:
            own_out(c).start()
            mates(lambda j: ret(c, which * plane + j).start())
        else:
            each(0, plane, lambda i: ret(c, which * plane + lax.rem(me_j + i, plane)).start())

    def near_batch(own, later=False):
        which = me_z if own else 1 - me_z
        at = pl.ds(pl.multiple_of(which * plane_rows, plane_rows), plane_rows)
        for c in range(PARTS):
            landed(received.at[at, part(c)], go_recv.at[1 if own else 0, c])

        def send(c):
            if not later:
                near_return(c, own)

        expert(received.at[at], results.at[at], send)

    def far_batch(k, inner_side):
        for c in range(PARTS):
            landed(far_received.at[k, :, part(c)], fgo_recv.at[k, c])

        def send(c):
            if inner_side:
                far_own_out(k, c).start()
            else:
                far_ret(k, c, me_j).start()
            mates(lambda j: far_ret(k, c, j).start())

        expert(far_received.at[k], far_results.at[k], send)

    def summed(slot, block):
        return jnp.dot(shares[slot, 0], block, preferred_element_type=jnp.float32) + jnp.dot(
            shares[slot, 1], block, preferred_element_type=jnp.float32
        )

    def far_sums(k):
        for c in range(PARTS):
            landed(far_returned.at[k, :, part(c)], fret_recv.at[k, c])
            partial[k, :, cut(c)] = summed(1 + k, far_returned[k, :, cut(c)]).astype(jnp.bfloat16)
            sum_out(k, c).start()

    def near_sums():
        for c in range(PARTS):
            landed(returned.at[:, part(c)], ret_recv.at[c])
            total[:, cut(c)] = mid[:, cut(c)].astype(jnp.float32) + summed(0, returned[:, cut(c)])

    for load in loads:
        load.wait()

    @pl.when(inside == 1)
    def _():
        with jax.named_scope("go"):
            for c in range(PARTS):
                spread(c)
                cross(c).start()
        with jax.named_scope("d1"):
            far_spread(0, True)
        with jax.named_scope("own"):
            near_batch(True)
        with jax.named_scope("d2"):
            far_spread(1, True)
        with jax.named_scope("ac"):
            for c in range(PARTS):
                across(c)
        with jax.named_scope("mate"):
            near_batch(False, True)
        with jax.named_scope("rt"):
            for c in range(PARTS):
                near_return(c, False)
        with jax.named_scope("b1"):
            far_batch(0, True)
        with jax.named_scope("b2"):
            far_batch(1, True)
        with jax.named_scope("s1"):
            far_sums(0)
        with jax.named_scope("s2"):
            far_sums(1)
        with jax.named_scope("near"):
            near_sums()

    @pl.when(inside == 0)
    def _():
        with jax.named_scope("go"):
            for c in range(PARTS):
                spread(c)
                across(c)
            for c in range(PARTS):
                cross(c).start()
        with jax.named_scope("own"):
            near_batch(True)
        with jax.named_scope("d1"):
            far_spread(0, False)
        with jax.named_scope("b1"):
            far_batch(0, False)
        with jax.named_scope("d2"):
            far_spread(1, False)
        with jax.named_scope("b2"):
            far_batch(1, False)
        with jax.named_scope("mate"):
            near_batch(False)
        with jax.named_scope("near"):
            near_sums()

    with jax.named_scope("end"):
        for c in range(PARTS):
            sum_here(c)
            out_ref[:, cut(c)] = (total[:, cut(c)] + inbox[:, cut(c)].astype(jnp.float32)).astype(
                jnp.bfloat16
            )

    with jax.named_scope("drain"):
        for n in range(2):
            for t in range(2):
                table(t, n, 1 - inside).wait_send()

        def gone(ref, sem):
            remote(ref, ref, sem, sum_recv.at[0], on_line(near_z)).wait_send()

        gone(staged.at[:, :, pl.ds(0, others)], send_sem)
        gone(outs.at[:, pl.ds(0, (count_sp - 1) * rows), :], back_send)
        gone(buffer.at[pl.ds(0, (half - 1) * capacity)], go_send)
        gone(results.at[pl.ds(0, (half - 1) * capacity)], ret_send)
        gone(far_buffer.at[:, pl.ds(0, (plane - 1) * capacity)], fgo_send)
        gone(xin, far_send)

        @pl.when(inside == 0)
        def _():
            gone(far_results, fret_send)

        @pl.when(inside == 1)
        def _():
            gone(far_results.at[:, pl.ds(0, (plane - 1) * capacity)], fret_send)
            gone(far, relay_send)
            gone(partial, sum_send)


def kernels_on_device(
    residual,
    query_maps,
    key_maps,
    value_rows,
    lambdas,
    head_gain,
    out_weight,
    ffn_gain,
    routes,
    route_weights,
    expert_gate,
    expert_up,
    expert_down,
):
    count_sp = lax.axis_size("sp")
    count_dp = lax.axis_size("dp")
    experts_all = count_sp * count_dp
    rows = residual.shape[1]
    capacity = max(2, 4 * rows // experts_all)
    if capacity % 16 or count_sp % LINE:
        return on_device(
            residual,
            query_maps,
            key_maps,
            value_rows,
            lambdas,
            head_gain,
            out_weight,
            ffn_gain,
            routes,
            route_weights,
            expert_gate,
            expert_up,
            expert_down,
        )
    heads_here = HEADS // count_sp
    half = experts_all // 2
    plane = half // 2
    slots = half * capacity
    vmem = pl.BlockSpec(memory_space=pltpu.VMEM)
    hbm = pl.BlockSpec(memory_space=pl.ANY)
    dma = pltpu.SemaphoreType.DMA
    bf16, f32 = jnp.bfloat16, jnp.float32
    length = rows * count_sp
    width = expert_gate.shape[2]
    top = routes.shape[2]
    out = pl.pallas_call(
        functools.partial(layer_kernel, count_sp, count_dp, capacity),
        out_shape=jax.ShapeDtypeStruct((rows, D), bf16),
        in_specs=[pl.BlockSpec(memory_space=pltpu.SMEM), hbm, hbm, hbm, vmem, vmem, hbm, vmem]
        + [vmem, vmem, hbm, hbm, hbm],
        out_specs=vmem,
        scratch_shapes=[
            pltpu.VMEM((3, rows, D), bf16),
            pltpu.VMEM((heads_here, length, VD), bf16),
            pltpu.VMEM((heads_here, length, VD), bf16),
            pltpu.VMEM((heads_here, length, VD), bf16),
            pltpu.VMEM((heads_here, length, VD), bf16),
            pltpu.VMEM((rows, HEADS * VD), bf16),
            pltpu.VMEM(out_weight.shape, bf16),
            pltpu.VMEM((rows, D), bf16),
            pltpu.VMEM((rows, D), bf16),
            pltpu.VMEM((2, top, rows), jnp.int32),
            pltpu.VMEM((2, top, rows), f32),
            pltpu.VMEM((3, slots, rows), bf16),
            pltpu.VMEM((3, 2, rows, slots), bf16),
            pltpu.VMEM((2, rows, D), bf16),
            pltpu.VMEM((2, rows, D), bf16),
            pltpu.VMEM((rows, D), bf16),
            pltpu.VMEM((rows, D), f32),
            pltpu.VMEM((slots, D), bf16),
            pltpu.VMEM((slots, D), bf16),
            pltpu.VMEM((slots, D), bf16),
            pltpu.VMEM((slots, D), bf16),
            pltpu.VMEM((2, slots // 2, D), bf16),
            pltpu.VMEM((2, slots // 2, D), bf16),
            pltpu.VMEM((2, slots // 2, D), bf16),
            pltpu.VMEM((2, slots, D), bf16),
            pltpu.VMEM((D, width), bf16),
            pltpu.VMEM((D, width), bf16),
            pltpu.VMEM((width, D), bf16),
            pltpu.VMEM((slots // 2, width), bf16),
            dma,
            dma((heads_here,)),
            dma((heads_here, count_sp)),
            dma((heads_here,)),
            dma,
            dma,
            dma,
            dma((3,)),
            dma((2, 2)),
            dma((2, 2)),
            dma,
            dma((2, PARTS)),
            dma,
            dma,
            dma((PARTS,)),
            dma,
            dma((2, PARTS)),
            dma,
            dma((PARTS,)),
            dma,
            dma((2, PARTS)),
            dma,
            dma((2, PARTS)),
            dma((3,)),
        ],
        compiler_params=pltpu.CompilerParams(
            collective_id=0, has_side_effects=True, vmem_limit_bytes=VMEM_LIMIT
        ),
    )(
        lambdas,
        query_maps[0],
        key_maps[0],
        value_rows[0],
        residual[0],
        head_gain.reshape(HEADS, VD),
        out_weight,
        ffn_gain.reshape(1, D),
        routes[0].T,
        route_weights[0].T,
        expert_gate[0],
        expert_up[0],
        expert_down[0],
    )
    return out[None]


def solution(mesh):
    return jax.shard_map(
        kernels_on_device,
        mesh=mesh,
        in_specs=(
            P("dp", "sp", None),
            P("dp", "sp", None),
            P("dp", "sp", None),
            P("dp", "sp", None),
            P(),
            P(),
            P(),
            P(),
            P("dp", "sp", None),
            P("dp", "sp", None),
            P(("sp", "dp"), None, None),
            P(("sp", "dp"), None, None),
            P(("sp", "dp"), None, None),
        ),
        out_specs=P("dp", "sp", None),
        check_vma=False,
    )
```

time: 144 us -> 126 us (0.88)
  Pallas kernels: 142 us -> 123 us
    pallas_call x2 -> x1, Pallas kernels: 142 us -> 123 us  [kernels_on_device(): pl.pallas_call(functools.partial(layer_kernel, count_sp, count_dp, capaci...]
where the time goes in v2:
time: 126 us; the launch traced here: 125 us
  Pallas kernels  123 us (98%)
  local copies, waits for them, and re-layouts  1.88 us (1%)
    pallas_call x1, Pallas kernels, kernels_on_device(): pl.pallas_call(functools.partial(layer_kernel, count_sp, count_dp, capaci...  123 us

profile of v2, /device:TPU:0, one launch (start us, length us, event | category | flops | bytes accessed | tf_op | source)
XLA Modules:
  0.0 124.7 jit_solution(16057292457891546883)
XLA Ops:
  0.0 122.9 %shard_map.127 = bf16[128,2048]{1,0:T(8,128)(2,1)} custom-call(f32[16]{0:T(128)} %lam_ref.1, bf16[128,2048]{1,0:T(8,128)(2,1)} %bitcast.20, bf16[128,2048]{1,0:T(8,128)(2,1)} %bitcast.21, bf16[128,2048]{1,0:T(8,128)(2,1)} %bitcast.22, bf16[128,2048]{1,0:T(8,128)(2,1)} %bitcast.23, f32[16,128]{1,0:T(8,128)} %bitcast.24, bf16[2048,2048]{1,0:T(8,128)(2,1)} %ow_hbm.1, ...), custom_call_target="tpu_custom_call" | custom-call | tf_op jit(solution)/shard_map/pallas_call | solution.py:777
  122.9 1.9 %copy.15 = bf16[1,128,2048]{2,1,0:T(8,128)(2,1)} copy(bf16[1,128,2048]{2,1,0:T(8,128)(2,1)} %bitcast.19) | data formatting | bytes 1048576

commit v3 on v2

--- a/solution.py
+++ b/solution.py
@@ -310,7 +310,13 @@
             device_id_type=MESH,
         )
 
-    weight_copy = pltpu.make_async_copy(ow_hbm, ow, ow_sem)
+    def weight_copy(i):
+        h, member = i // count_sp, lax.rem(i, count_sp)
+        given = pl.ds(pl.multiple_of((member * heads_here + h) * VD, VD), VD)
+        return pltpu.make_async_copy(
+            ow_hbm.at[given], ow.at[pl.ds(pl.multiple_of(i * VD, VD), VD)], ow_sem
+        )
+
     loads = [
         pltpu.make_async_copy(src, dst, weight_sem.at[j])
         for j, (src, dst) in enumerate(((gate_hbm, gate), (up_hbm, up), (down_hbm, down)))
@@ -332,7 +338,12 @@
     for n in range(2):
         for t in range(2):
             table(t, n, 1 - inside).start()
-    weight_copy.start()
+
+    def start_weight(i, carry):
+        weight_copy(i).start()
+        return carry
+
+    lax.fori_loop(0, HEADS, start_weight, 0)
     for load in loads:
         load.start()
 
@@ -348,79 +359,102 @@
 
     set_tables(0, routes_ref[...], weights_ref[...])
 
-    def returning(h, p, d):
-        dst_cols = pl.ds(pl.multiple_of((me_sp * heads_here + h) * VD, VD), VD)
-        return pltpu.make_async_remote_copy(
-            src_ref=outs.at[h, pl.ds(pl.multiple_of(p * rows, rows), rows), :],
-            dst_ref=att.at[:, dst_cols],
-            send_sem=back_send,
-            recv_sem=back_recv,
-            device_id={"sp": p},
-            device_id_type=MESH,
-        )
+    def returning(h, p):
+        dst_cols = pl.ds(pl.multiple_of((h * count_sp + me_sp) * VD, VD), VD)
+        held = outs.at[h, pl.ds(pl.multiple_of(p * rows, rows), rows), :]
+
+        @pl.when(p != me_sp)
+        def _():
+            pltpu.make_async_remote_copy(
+                src_ref=held,
+                dst_ref=att.at[:, dst_cols],
+                send_sem=back_send,
+                recv_sem=back_recv.at[h],
+                device_id={"sp": p},
+                device_id_type=MESH,
+            ).start()
+
+        @pl.when(p == me_sp)
+        def _():
+            pltpu.make_async_copy(held, att.at[:, dst_cols], back_recv.at[h]).start()
 
     factor = HD ** (-0.5) * math.log2(math.e)
     lanes = lax.broadcasted_iota(jnp.int32, (rows, VD), 1)
+    def attend(h, p):
+        head = me_sp * heads_here + h
+        lam = lam_ref[head]
+        gain = gain_ref[pl.ds(head, 1), :]
+        at = pl.ds(pl.multiple_of(p * rows, rows), rows)
+        q = qh[h, at, :]
+        zero = jnp.zeros_like(q)
+        both = jnp.concatenate(
+            [jnp.where(lanes < HD, q, zero), jnp.where(lanes < HD, zero, q)], axis=0
+        )
+        scores = lax.dot_general(
+            both, kh[h], (((1,), (1,)), ((), ())), preferred_element_type=jnp.float32
+        )
+        top = jnp.max(scores, axis=1, keepdims=True)
+        e = jnp.exp2((scores - top) * factor)
+        norm = jnp.sum(e, axis=1, keepdims=True)
+        norm_1, norm_2 = norm[:rows], norm[rows:]
+        share = lam * norm_1 / norm_2
+        mixed = (e[:rows] - share * e[rows:]).astype(jnp.bfloat16)
+        head_out = jnp.dot(mixed, vh[h], preferred_element_type=jnp.float32) / norm_1
+        normed = head_out * lax.rsqrt(jnp.mean(head_out * head_out, axis=-1, keepdims=True) + eps)
+        return (normed * gain * 0.8).astype(jnp.bfloat16)
+
     for h in range(heads_here):
+
+        def step(i, carry, h=h):
+            places = []
+            for n in range(2):
+                d = lax.rem(2 * i + n + count_sp // 2, count_sp)
+                p = lax.rem(me_sp + count_sp - d, count_sp)
+                at = pl.ds(pl.multiple_of(p * rows, rows), rows)
+                landed(qh.at[h, at, :], query_recv.at[h, d])
+                places.append((p, at))
+            blocks = [attend(h, p) for p, _ in places]
+            for (p, at), block in zip(places, blocks):
+                outs[h, at, :] = block
+            for p, _ in places:
+                returning(h, p)
+            return carry
+
         with jax.named_scope("kv"):
             landed(kh.at[h], key_recv.at[h])
             landed(vh.at[h], value_recv.at[h])
-        head = me_sp * heads_here + h
-        lam = lam_ref[head]
-        gain = gain_ref[pl.ds(head, 1), :]
-
-        def attend(p, h=h, lam=lam, gain=gain):
-            at = pl.ds(pl.multiple_of(p * rows, rows), rows)
-            q = qh[h, at, :]
-            zero = jnp.zeros_like(q)
-            both = jnp.concatenate(
-                [jnp.where(lanes < HD, q, zero), jnp.where(lanes < HD, zero, q)], axis=0
-            )
-            scores = lax.dot_general(
-                both, kh[h], (((1,), (1,)), ((), ())), preferred_element_type=jnp.float32
-            )
-            top = jnp.max(scores, axis=1, keepdims=True)
-            e = jnp.exp2((scores - top) * factor)
-            norm = jnp.sum(e, axis=1, keepdims=True)
-            norm_1, norm_2 = norm[:rows], norm[rows:]
-            share = lam * norm_1 / norm_2
-            mixed = (e[:rows] - share * e[rows:]).astype(jnp.bfloat16)
-            head_out = jnp.dot(mixed, vh[h], preferred_element_type=jnp.float32) / norm_1
-            normed = head_out * lax.rsqrt(
-                jnp.mean(head_out * head_out, axis=-1, keepdims=True) + eps
-            )
-            return (normed * gain * 0.8).astype(jnp.bfloat16)
-
-        def step(i, carry, h=h, attend=attend):
-            d = 1 + lax.rem(i + count_sp // 2 - 1, count_sp - 1)
-            p = lax.rem(me_sp + count_sp - d, count_sp)
-            outgoing(1, h, d).wait_recv()
-            outs[h, pl.ds(pl.multiple_of(p * rows, rows), rows), :] = attend(p)
-            returning(h, p, d).start()
-            return carry
-
         with jax.named_scope("steps"):
-            lax.fori_loop(0, count_sp - 1, step, 0)
-        local_copy(1, h).wait()
-        with jax.named_scope("mine"):
-            att[:, pl.ds(pl.multiple_of(head * VD, VD), VD)] = attend(me_sp)
+            lax.fori_loop(0, count_sp // 2, step, 0)
 
     for slot in range(2):
         for t in range(2):
             table(t, 0, slot).wait_recv()
         set_tables(1 + slot, routes_far[slot], weights_far[slot])
 
-    weight_copy.wait()
+    landed(ow, ow_sem)
     others = (count_sp - 1) * heads_here * VD
+    tile = 512
+    deep = count_sp * VD
+
+    def projection(h, cols):
+        heads = slice(h * deep, (h + 1) * deep)
+        return jnp.dot(att[:, heads], ow[heads, cols], preferred_element_type=jnp.float32)
+
+    for h in range(heads_here - 1):
+        landed(att.at[:, pl.ds(h * deep, deep)], back_recv.at[h])
+        for j in range(D // tile):
+            cols = slice(j * tile, (j + 1) * tile)
+            so_far = residual_ref[:, cols].astype(jnp.float32) if h == 0 else total[:, cols]
+            total[:, cols] = so_far + projection(h, cols)
+    last = heads_here - 1
     with jax.named_scope("back"):
-        landed(att.at[:, pl.ds(0, others)], back_recv)
-
-    tile = 512
+        landed(att.at[:, pl.ds(last * deep, deep)], back_recv.at[last])
+
     square = jnp.zeros((rows, 1), jnp.float32)
     for j in range(D // tile):
         cols = slice(j * tile, (j + 1) * tile)
-        projected = jnp.dot(att[...], ow[:, cols], preferred_element_type=jnp.float32)
-        middle = (residual_ref[:, cols].astype(jnp.float32) + projected).astype(jnp.bfloat16)
+        so_far = residual_ref[:, cols].astype(jnp.float32) if last == 0 else total[:, cols]
+        middle = (so_far + projection(last, cols)).astype(jnp.bfloat16)
         mid[:, cols] = middle
         wide = middle.astype(jnp.float32)
         square = square + jnp.sum(wide * wide, axis=1, keepdims=True)
@@ -677,6 +711,7 @@
             for c in range(PARTS):
                 spread(c)
                 across(c)
+        with jax.named_scope("cr"):
             for c in range(PARTS):
                 cross(c).start()
         with jax.named_scope("own"):
@@ -815,7 +850,7 @@
             dma((heads_here, count_sp)),
             dma((heads_here,)),
             dma,
-            dma,
+            dma((heads_here,)),
             dma,
             dma((3,)),
             dma((2, 2)),

time: 126 us -> 125 us (level)
  no operation moved by 1% of the time
where the time goes in v3:
time: 125 us; the launch traced here: 124 us
  Pallas kernels  122 us (98%)
  local copies, waits for them, and re-layouts  1.88 us (2%)
    pallas_call x1, Pallas kernels, kernels_on_device(): pl.pallas_call(functools.partial(layer_kernel, count_sp, count_dp, capaci...  122 us

profile of v3, /device:TPU:0, one launch (start us, length us, event | category | flops | bytes accessed | tf_op | source)
XLA Modules:
  0.0 123.9 jit_solution(5563454059875680393)
XLA Ops:
  0.0 122.0 %shard_map.127 = bf16[128,2048]{1,0:T(8,128)(2,1)} custom-call(f32[16]{0:T(128)} %lam_ref.1, bf16[128,2048]{1,0:T(8,128)(2,1)} %bitcast.20, bf16[128,2048]{1,0:T(8,128)(2,1)} %bitcast.21, bf16[128,2048]{1,0:T(8,128)(2,1)} %bitcast.22, bf16[128,2048]{1,0:T(8,128)(2,1)} %bitcast.23, f32[16,128]{1,0:T(8,128)} %bitcast.24, bf16[2048,2048]{1,0:T(8,128)(2,1)} %ow_hbm.1, ...), custom_call_target="tpu_custom_call" | custom-call | tf_op jit(solution)/shard_map/pallas_call | solution.py:812
  122.0 1.9 %copy.15 = bf16[1,128,2048]{2,1,0:T(8,128)(2,1)} copy(bf16[1,128,2048]{2,1,0:T(8,128)(2,1)} %bitcast.19) | data formatting | bytes 1048576

commit v4 on v3

--- a/solution.py
+++ b/solution.py
@@ -246,6 +246,7 @@
     last_z = 3 - 3 * side
     width = gate.shape[1]
     span = D // PARTS
+    chunk = width // 2
 
     def coords(p):
         return {"sp": (base + p) // count_dp, "dp": lax.rem(base + p, count_dp)}
@@ -609,13 +610,13 @@
 
     def expert(source, target, send):
         def make_hidden(j, carry):
-            cols = pl.ds(pl.multiple_of(j * 256, 256), 256)
+            cols = pl.ds(pl.multiple_of(j * chunk, chunk), chunk)
             gate_part = jnp.dot(source[...], gate[:, cols], preferred_element_type=jnp.float32)
             up_part = jnp.dot(source[...], up[:, cols], preferred_element_type=jnp.float32)
             hidden[:, cols] = (jax.nn.silu(gate_part) * up_part).astype(jnp.bfloat16)
             return carry
 
-        lax.fori_loop(0, width // 256, make_hidden, 0)
+        lax.fori_loop(0, width // chunk, make_hidden, 0)
         for c in range(PARTS):
             target[:, cut(c)] = jnp.dot(
                 hidden[...], down[:, cut(c)], preferred_element_type=jnp.float32

time: 125 us -> 124 us (level)
  no operation moved by 1% of the time
where the time goes in v4:
time: 124 us
  Pallas kernels  122 us (98%)
  local copies, waits for them, and re-layouts  1.88 us (2%)
    pallas_call x1, Pallas kernels, kernels_on_device(): pl.pallas_call(functools.partial(layer_kernel, count_sp, count_dp, capaci...  122 us

profile of v4, /device:TPU:0, one launch (start us, length us, event | category | flops | bytes accessed | tf_op | source)
XLA Modules:
  0.0 123.6 jit_solution(13318526316517688589)
XLA Ops:
  0.0 121.7 %shard_map.127 = bf16[128,2048]{1,0:T(8,128)(2,1)} custom-call(f32[16]{0:T(128)} %lam_ref.1, bf16[128,2048]{1,0:T(8,128)(2,1)} %bitcast.20, bf16[128,2048]{1,0:T(8,128)(2,1)} %bitcast.21, bf16[128,2048]{1,0:T(8,128)(2,1)} %bitcast.22, bf16[128,2048]{1,0:T(8,128)(2,1)} %bitcast.23, f32[16,128]{1,0:T(8,128)} %bitcast.24, bf16[2048,2048]{1,0:T(8,128)(2,1)} %ow_hbm.1, ...), custom_call_target="tpu_custom_call" | custom-call | tf_op jit(solution)/shard_map/pallas_call | solution.py:813
  121.7 1.9 %copy.15 = bf16[1,128,2048]{2,1,0:T(8,128)(2,1)} copy(bf16[1,128,2048]{2,1,0:T(8,128)(2,1)} %bitcast.19) | data formatting | bytes 1048576
